TPU v7x, 32 devices: a whole 2x2x4 slice. The times are simulated.
32 devices in a mesh: dp: 4 (over y, x), kv: 4 (over z), tp: 2 (over core).
Axes of the slice: x: 2, y: 2, z: 4, core: 2. Of those that a mesh axis runs over, the one named last changes fastest.
Arguments:
- hidden: bfloat16 [2048, 16], P(('kv', 'tp'), 'dp'), parts along dimension 1, may hold values from -20 to 20
- mixer_gain: float32 [2048], replicated, may hold values from 0.1 to 1.9
- gate_proj: bfloat16 [2048, 64, 64], P(None, 'kv', 'tp'), may hold values from -0.125 to 0.125
- inner_proj: bfloat16 [2048, 64, 64], P(None, 'kv', 'tp'), may hold values from -0.125 to 0.125
- input_proj: bfloat16 [2048, 1024], P(None, 'kv'), may hold values from -0.125 to 0.125
- output_proj: bfloat16 [2048, 1024], P(None, 'kv'), may hold values from -0.125 to 0.125
- step_proj: bfloat16 [2048, 64], replicated, may hold values from -0.125 to 0.125
- step_bias: float32 [64], replicated, may hold values from -3 to -0.5
- decay_log: float32 [64], replicated, may hold values from -3 to 1
- skip_gain: float32 [64], replicated, may hold values from 0.3 to 1.5
- taps_inner: float32 [4, 64, 64], P(None, None, 'tp'), may hold values from -3 to 3
- taps_input: float32 [4, 1024], replicated, may hold values from -3 to 3
- taps_output: float32 [4, 1024], replicated, may hold values from -3 to 3
- recent_inner: bfloat16 [16, 3, 64, 64], P(('dp', 'kv'), None, None, 'tp'), parts along dimension 0, may hold values from -6 to 6
- recent_input: bfloat16 [16, 3, 1024], P(('dp', 'kv')), parts along dimension 0, may hold values from -6 to 6
- recent_output: bfloat16 [16, 3, 1024], P(('dp', 'kv')), parts along dimension 0, may hold values from -6 to 6
- states: float32 [16, 64, 64, 128], P(('dp', 'kv'), None, 'tp'), parts along dimension 0, may hold values from -4 to 4
- block_inner: bfloat16 [16, 128, 64, 64], P(('dp', 'kv'), None, None, 'tp'), parts along dimension 0, may hold values from -6 to 6
- block_input: bfloat16 [16, 128, 1024], P(('dp', 'kv')), parts along dimension 0, may hold values from -4 to 4
- block_decay: float32 [16, 128, 64], P(('dp', 'kv')), parts along dimension 0
- lengths: int32 [16], P(('dp', 'kv')), parts along dimension 0, may hold values from 1 to 128, 170 in all
- norm_gain: float32 [64, 64], P(None, 'tp'), may hold values from 0.1 to 1.9
- mixer_out: bfloat16 [64, 64, 2048], P('kv', 'tp'), may hold values from -0.125 to 0.125
- channel_gain: float32 [2048], replicated, may hold values from 0.1 to 1.9
- expand_gate: bfloat16 [2048, 5632], P(None, ('kv', 'tp')), may hold values from -0.125 to 0.125
- expand_value: bfloat16 [2048, 5632], P(None, ('kv', 'tp')), may hold values from -0.125 to 0.125
- reduce_proj: bfloat16 [5632, 2048], P(('kv', 'tp')), may hold values from -0.109375 to 0.109375
Outputs:
- layer_out: bfloat16 [2048, 16], P(('kv', 'tp'), 'dp'), parts along dimension 1
There are 4 independent parts, one for each index of `dp`. A program takes and returns all parts, laid end to end along the dimension named above; an argument that names none is the same for every part. Nothing has to cross between parts.
All inputs are finite; a program needn't handle non-finite values. No bound on the sum of `lengths` on one device may be relied on, other than what follows from the above.
Results may differ from a plain program's by a relative error of at most 0.01.
Values may be sent and summed in bfloat16 or wider, within the bound.
No kernel may reach another device: no remote copies, remote signals or barrier semaphores. Data moves between devices by JAX's collectives and lax.ppermute only.
A program may use at most 64 MiB of HBM per device.

v0:
```python
import jax
import jax.numpy as jnp
from jax import lax
from jax.sharding import PartitionSpec as P

MIXER_HEADS = 64
HEAD_DIM = 64
GROUPS = 8
STATE = 128
OPEN_BLOCK_SPAN = 128
epsilon = 1e-05


def short_conv(recent, newest, taps):
    window = jnp.concatenate(
        [recent.astype(jnp.float32), newest.astype(jnp.float32)[:, None]], axis=1
    )
    return jax.nn.silu(jnp.sum(window * taps[None], axis=1))


def shards(
    hidden,
    mixer_gain,
    gate_proj,
    inner_proj,
    input_proj,
    output_proj,
    step_proj,
    step_bias,
    decay_log,
    skip_gain,
    taps_inner,
    taps_input,
    taps_output,
    recent_inner,
    recent_input,
    recent_output,
    states,
    block_inner,
    block_input,
    block_decay,
    lengths,
    norm_gain,
    mixer_out,
    channel_gain,
    expand_gate,
    expand_value,
    reduce_proj,
):
    rows_own = hidden.shape[0]
    seq_all = hidden.shape[1]
    seq_dev = states.shape[0]
    half_dim = states.shape[2]
    width = rows_own * lax.axis_size("kv") * lax.axis_size("tp")
    offset = (lax.axis_index("kv") * lax.axis_size("tp") + lax.axis_index("tp")) * rows_own
    own_start = lax.axis_index("kv") * seq_dev
    whole_rows = lax.all_gather(hidden, ("kv", "tp"), axis=0, tiled=True)
    whole_f = whole_rows.astype(jnp.float32)
    rms_in = lax.rsqrt(jnp.mean(whole_f * whole_f, axis=0) + epsilon)
    normed_in = (whole_f * mixer_gain[:, None]).astype(jnp.bfloat16)
    gate_part = (
        rms_in[:, None, None]
        * jnp.einsum("ds,dhp->shp", normed_in, gate_proj, preferred_element_type=jnp.float32)
    ).astype(jnp.bfloat16)
    inner_part = (
        rms_in[:, None, None]
        * jnp.einsum("ds,dhp->shp", normed_in, inner_proj, preferred_element_type=jnp.float32)
    ).astype(jnp.bfloat16)
    input_part = (
        rms_in[:, None]
        * jnp.einsum("ds,dk->sk", normed_in, input_proj, preferred_element_type=jnp.float32)
    ).astype(jnp.bfloat16)
    output_part = (
        rms_in[:, None]
        * jnp.einsum("ds,dk->sk", normed_in, output_proj, preferred_element_type=jnp.float32)
    ).astype(jnp.bfloat16)
    own_cols = lax.dynamic_slice_in_dim(normed_in, own_start, seq_dev, 1)
    own_rms = lax.dynamic_slice_in_dim(rms_in, own_start, seq_dev, 0)
    step_pre = (
        own_rms[:, None]
        * jnp.einsum("ds,dh->sh", own_cols, step_proj, preferred_element_type=jnp.float32)
    ).astype(jnp.bfloat16)
    gate_pre, inner_pre, input_pre, output_pre = (
        lax.all_to_all(gate_part, "kv", split_axis=0, concat_axis=1, tiled=True),
        lax.all_to_all(inner_part, "kv", split_axis=0, concat_axis=1, tiled=True),
        lax.all_to_all(input_part, "kv", split_axis=0, concat_axis=1, tiled=True),
        lax.all_to_all(output_part, "kv", split_axis=0, concat_axis=1, tiled=True),
    )
    conv_inner = short_conv(recent_inner, inner_pre, taps_inner)
    conv_input = short_conv(recent_input, input_pre, taps_input)
    conv_output = short_conv(recent_output, output_pre, taps_output).astype(jnp.bfloat16)
    step = jax.nn.softplus(step_pre.astype(jnp.float32) + step_bias[None, :])
    new_decay = -jnp.exp(decay_log)[None, :] * step
    per_group = MIXER_HEADS // GROUPS
    live = (jnp.arange(OPEN_BLOCK_SPAN, dtype=jnp.int32)[None, :] < lengths[:, None]).astype(
        jnp.float32
    )
    masked = block_decay * live[:, :, None]
    cached = jnp.sum(masked, axis=1)
    tail = new_decay[:, None, :] + cached[:, None, :] - jnp.cumsum(masked, axis=1)
    total = new_decay + cached
    readout = conv_output.reshape(seq_dev, GROUPS, STATE)
    score = jnp.einsum(
        "sgn,sjgn->sgj",
        readout,
        block_input.reshape(seq_dev, OPEN_BLOCK_SPAN, GROUPS, STATE),
        preferred_element_type=jnp.float32,
    )
    score_heads = jnp.repeat(score, per_group, axis=1)
    weight = (live[:, None, :] * jnp.exp(jnp.swapaxes(tail, 1, 2)) * score_heads).astype(
        jnp.bfloat16
    )
    from_block = jnp.einsum(
        "shj,sjhp->shp", weight, block_inner, preferred_element_type=jnp.float32
    )
    readout_f = readout.astype(jnp.float32)
    grouped = states.reshape(seq_dev, GROUPS, per_group, half_dim, STATE)
    from_state = jnp.einsum(
        "sgn,sgrpn->sgrp", readout_f, grouped, precision=lax.Precision.HIGHEST
    ).reshape(seq_dev, MIXER_HEADS, half_dim)
    own_score = jnp.repeat(
        jnp.sum(readout_f * conv_input.reshape(seq_dev, GROUPS, STATE), axis=-1), per_group, axis=1
    )
    mix = (
        from_block
        + jnp.exp(total)[:, :, None] * from_state
        + (own_score * step)[:, :, None] * conv_inner
        + skip_gain[None, :, None] * conv_inner
    )
    gated_raw = mix * jax.nn.silu(gate_pre.astype(jnp.float32))
    part_squares = jnp.sum(gated_raw * gated_raw, axis=(1, 2))
    gated = (gated_raw * norm_gain[None]).astype(jnp.bfloat16)
    placed = lax.dynamic_update_slice_in_dim(
        jnp.zeros((seq_all,), jnp.float32), part_squares, own_start, 0
    )
    gate_squares = lax.psum(placed, ("kv", "tp"))
    rms_gate = lax.rsqrt(gate_squares / (MIXER_HEADS * HEAD_DIM) + epsilon)
    by_head = lax.all_to_all(gated, "kv", split_axis=1, concat_axis=0, tiled=True)
    columns = mixer_out
    mixed_full = rms_gate[None, :] * lax.psum(
        jnp.einsum("hpd,shp->ds", columns, by_head, preferred_element_type=jnp.float32),
        ("kv", "tp"),
    )
    mid_full = (whole_f + mixed_full).astype(jnp.bfloat16)
    mid = lax.dynamic_slice_in_dim(mid_full, offset, rows_own, 0)
    full_f = mid_full.astype(jnp.float32)
    mid_squares = jnp.sum(full_f * full_f, axis=0)
    normed_full = (full_f * channel_gain[:, None]).astype(jnp.bfloat16)
    gate_sum = jnp.einsum("ds,df->sf", normed_full, expand_gate, preferred_element_type=jnp.float32)
    value_sum = jnp.einsum(
        "ds,df->sf", normed_full, expand_value, preferred_element_type=jnp.float32
    )
    rms_mid = lax.rsqrt(mid_squares / width + epsilon)
    act = (jax.nn.silu(rms_mid[:, None] * gate_sum) * (rms_mid[:, None] * value_sum)).astype(
        jnp.bfloat16
    )
    columns = reduce_proj
    channel = lax.psum_scatter(
        jnp.einsum("fd,sf->ds", columns, act, preferred_element_type=jnp.float32),
        ("kv", "tp"),
        scatter_dimension=0,
        tiled=True,
    )
    return (mid.astype(jnp.float32) + channel).astype(jnp.bfloat16)


def solution(mesh):
    return jax.shard_map(
        shards,
        mesh=mesh,
        in_specs=(
            P(("kv", "tp"), "dp"),
            P(),
            P(None, "kv", "tp"),
            P(None, "kv", "tp"),
            P(None, "kv"),
            P(None, "kv"),
            P(),
            P(),
            P(),
            P(),
            P(None, None, "tp"),
            P(),
            P(),
            P(("dp", "kv"), None, None, "tp"),
            P(("dp", "kv"), None, None),
            P(("dp", "kv"), None, None),
            P(("dp", "kv"), None, "tp", None),
            P(("dp", "kv"), None, None, "tp"),
            P(("dp", "kv"), None, None),
            P(("dp", "kv"), None, None),
            P(("dp", "kv")),
            P(None, "tp"),
            P("kv", "tp", None),
            P(),
            P(None, ("kv", "tp")),
            P(None, ("kv", "tp")),
            P(("kv", "tp"), None),
        ),
        out_specs=P(("kv", "tp"), "dp"),
        check_vma=False,
    )
```

profile of v0, /device:TPU:0, one launch (start us, length us, event | category | flops | bytes accessed | tf_op | source)
XLA Modules:
  0.0 156.3 jit_solution(15144254045306652727)
XLA Ops:
  6.5 14.7 %all_gather.3 = bf16[2048,4]{0,1:T(4,128)(2,1)S(1)} all-gather(bf16[256,4]{0,1:T(4,128)(2,1)} %param.27), channel_id=1, replica_groups=mesh['dp'=4,'kv'=4,'tp'=2] {'kv','tp'}, dimensions={0}, use_global_device_ids=true | all-gather | bytes 18432 | tf_op jit(solution)/shard_map/all_gather | solution.py:57
  21.3 0.8 fusion.15
  22.1 1.4 fusion.7
  25.4 3.4 %all-to-all-start = ((bf16[4,2,128]{2,1,0:T(2,128)(2,1)}), bf16[4,2,128]{2,1,0:T(2,128)(2,1)S(1)}, u32[]{:S(2)}, u32[]{:S(2)}) async-start(bf16[4,2,128]{2,1,0:T(2,128)(2,1)} %reshape.385), calls=%async_computation | async-start | bytes 4096 | tf_op jit(solution)/shard_map/all_to_all | solution.py:87
  29.5 1.4 fusion.6
  31.0 3.1 %fusion.1 = bf16[4,16,32]{2,0,1:T(4,128)(2,1)S(1)} fusion(bf16[2048,16,32]{0,2,1:T(8,128)(2,1)} %param.29, bf16[2048,4]{0,1:T(4,128)(2,1)S(1)} %get-tuple-element.16, f32[4]{0:T(128)S(1)} %add_rsqrt_fusion.2), kind=kOutput, calls=%fused_computation.5 | convolution fusion | flops 8392704 | bytes 2117648 | tf_op jit(solution)/shard_map/ds,dhp->shp/dot_general | solution.py:63
  34.1 1.5 fusion
  36.9 5.1 %all-to-all-start.1 = ((bf16[4,2,128]{2,1,0:T(2,128)(2,1)}), bf16[4,2,128]{2,1,0:T(2,128)(2,1)S(1)}, u32[]{:S(2)}, u32[]{:S(2)}) async-start(bf16[4,2,128]{2,1,0:T(2,128)(2,1)} %reshape.387), calls=%async_computation.1 | async-start | bytes 4096 | tf_op jit(solution)/shard_map/all_to_all | solution.py:86
  43.3 0.7 reshape.381
  44.0 0.7 reshape.383
  45.0 2.5 %all-to-all-done.1 = bf16[4,2,128]{2,1,0:T(2,128)(2,1)S(1)} async-done(((bf16[4,2,128]{2,1,0:T(2,128)(2,1)}), bf16[4,2,128]{2,1,0:T(2,128)(2,1)S(1)}, u32[]{:S(2)}, u32[]{:S(2)}) %all-to-all-start.1) | async-done | bytes 2080 | tf_op jit(solution)/shard_map/all_to_all | solution.py:86
  47.5 3.2 %all-to-all-start.2 = ((bf16[4,2,256]{2,1,0:T(2,128)(2,1)}), bf16[4,2,256]{2,1,0:T(2,128)(2,1)S(1)}, u32[]{:S(2)}, u32[]{:S(2)}) async-start(bf16[4,2,256]{2,1,0:T(2,128)(2,1)} %reshape.383), calls=%async_computation.2 | async-start | bytes 8192 | tf_op jit(solution)/shard_map/all_to_all | solution.py:85
  50.8 0.8 multiply_reduce_fusion.3
  52.2 3.4 %fusion.43 = f32[8,1,8,32]{3,1,2,0:T(1,128)S(1)} fusion(f32[8,8,32,128]{3,2,1,0:T(8,128)} %bitcast.136, bf16[8,128,1,1]{1,0,2,3:T(8,128)(2,1)S(1)} %get-tuple-element.17), kind=kOutput, calls=%fused_computation.72 | convolution fusion | flops 3145728 | bytes 1058816 | tf_op jit(solution)/shard_map/sgn,sgrpn->sgrp/dot_general | solution.py:118
  55.6 1.8 %fusion.57 = (f32[64]{0:T(128)S(1)}, f32[64]{0:T(128)S(1)}, f32[64]{0:T(128)S(1)}) fusion(f32[64]{0:T(128)} %get-tuple-element.13, f32[64]{0:T(128)} %param.35, f32[64]{0:T(128)S(1)} %broadcast_in_dim.11, f32[64]{0:T(128)} %param.34, bf16[2048,64]{0,1:T(8,128)(2,1)} %param.33, bf16[2048,4]{0,1:T(4,128)(2,1)S(1)} %get-tuple-element.16, s32[]{:T(128)S(6)} %select_n.13, ...), kind=kOutput, calls=%fused_computation.90 | convolution fusion | flops 263040 | bytes 272392 | tf_op jit(solution)/shard_map/ds,dh->sh/dot_general | solution.py:81
  57.4 0.8 fusion.19
  58.2 5.1 %all-to-all-start.3 = ((bf16[4,2,256]{2,1,0:T(2,128)(2,1)}), bf16[4,2,256]{2,1,0:T(2,128)(2,1)S(1)}, u32[]{:S(2)}, u32[]{:S(2)}) async-start(bf16[4,2,256]{2,1,0:T(2,128)(2,1)} %reshape.381), calls=%async_computation.3 | async-start | bytes 8192 | tf_op jit(solution)/shard_map/all_to_all | solution.py:84
  63.3 1.4 multiply_reduce_fusion
  65.0 3.9 %all-to-all-done.3 = bf16[4,2,256]{2,1,0:T(2,128)(2,1)S(1)} async-done(((bf16[4,2,256]{2,1,0:T(2,128)(2,1)}), bf16[4,2,256]{2,1,0:T(2,128)(2,1)S(1)}, u32[]{:S(2)}, u32[]{:S(2)}) %all-to-all-start.3) | async-done | bytes 4128 | tf_op jit(solution)/shard_map/all_to_all | solution.py:84
  69.0 1.3 multiply_reduce_fusion.2
  70.5 0.7 reduce.14
  71.2 0.7 reshape.389
  71.9 3.2 %all-to-all-start.4 = ((bf16[4,2,256]{2,1,0:T(2,128)(2,1)}), bf16[4,2,256]{2,1,0:T(2,128)(2,1)S(1)}, u32[]{:S(2)}, u32[]{:S(2)}) async-start(bf16[4,2,256]{2,1,0:T(2,128)(2,1)} %reshape.389), calls=%async_computation.4 | async-start | bytes 8192 | tf_op jit(solution)/shard_map/all_to_all | solution.py:138
  75.2 0.8 dynamic_update_slice.3
  75.9 4.7 %all-to-all-done.4 = bf16[4,2,256]{2,1,0:T(2,128)(2,1)S(1)} async-done(((bf16[4,2,256]{2,1,0:T(2,128)(2,1)}), bf16[4,2,256]{2,1,0:T(2,128)(2,1)S(1)}, u32[]{:S(2)}, u32[]{:S(2)}) %all-to-all-start.4) | async-done | bytes 4128 | tf_op jit(solution)/shard_map/all_to_all | solution.py:138
  80.8 2.0 %convolution_bitcast_fusion.1 = f32[2048,4]{0,1:T(4,128)S(1)} fusion(bf16[16,32,2048]{2,1,0:T(8,128)(2,1)} %param.49, bf16[4,16,32]{2,1,0:T(8,128)(2,1)S(1)} %bitcast.141), kind=kOutput, calls=%fused_computation.1 | convolution fusion | flops 8388608 | bytes 2134016 | tf_op jit(solution)/shard_map/hpd,shp->ds/dot_general | solution.py:141
  82.8 26.3 %all-reduce = (f32[2048,4]{0,1:T(4,128)S(1)}, f32[4]{0:T(128)S(1)}) all-reduce(f32[2048,4]{0,1:T(4,128)S(1)} %convolution_bitcast_fusion.1, f32[4]{0:T(128)S(1)} %dynamic_update_slice.3), channel_id=1, replica_groups=mesh['dp'=4,'kv'=4,'tp'=2] {'kv','tp'}, use_global_device_ids=true, to_apply=%region_9.10 | all-reduce | flops 8196 | bytes 65568 | tf_op jit(solution)/shard_map/psum | solution.py:140
  109.3 2.7 %convolution_multiply_fusion.3 = f32[4,704]{1,0:T(4,128)S(1)} fusion(bf16[2048,704]{0,1:T(8,128)(2,1)} %param.51, bf16[2048,4]{0,1:T(4,128)(2,1)S(1)} %get-tuple-element.8, f32[2048]{0:T(1024)S(1)} %copy-done.4, f32[4]{0:T(128)S(1)} %add_rsqrt_fusion), kind=kOutput, calls=%fused_computation.8 | convolution fusion | flops 11561728 | bytes 2919440 | tf_op jit(solution)/shard_map/ds,df->sf/dot_general | solution.py:149
  112.0 3.5 %convolution_bitcast_fusion = f32[2048,4]{0,1:T(4,128)S(1)} fusion(bf16[704,2048]{1,0:T(8,128)(2,1)S(1)} %copy-done, bf16[2048,704]{0,1:T(8,128)(2,1)} %param.52, f32[4,704]{1,0:T(4,128)S(1)} %convolution_multiply_fusion.3, bf16[2048,4]{0,1:T(4,128)(2,1)S(1)} %get-tuple-element.8, f32[2048]{0:T(1024)S(1)} %copy-done.4, f32[4]{0:T(128)S(1)} %add_rsqrt_fusion), kind=kOutput, calls=%fused_computation | convolution fusion | flops 23112960 | bytes 5835792 | tf_op jit(solution)/shard_map/fd,sf->ds/dot_general | solution.py:159
  115.5 1.4 copy.71
  116.9 31.0 %reduce-scatter.4.cloned.1.call-done = f32[256,4]{1,0:T(8,128)} async-done(((f32[2048,4]{1,0:T(8,128)}), f32[256,4]{1,0:T(8,128)}) %reduce-scatter.4.cloned.1.call-update) | async-done | bytes 4112
  147.8 1.0 copy.72
  (63 shorter events, 7.1 us)
Async XLA Ops:
  6.5 105.4 %copy-start = (bf16[704,2048]{1,0:T(8,128)(2,1)S(1)}, bf16[704,2048]{1,0:T(8,128)(2,1)}, u32[]{:S(2)}) copy-start(bf16[704,2048]{1,0:T(8,128)(2,1)} %param.53) | copy-start | bytes 8650756
  23.5 13.3 %copy-start.5 = (f32[1,128,64]{1,2,0:T(8,128)S(1)}, f32[1,128,64]{1,2,0:T(8,128)}, u32[]{:S(2)}) copy-start(f32[1,128,64]{1,2,0:T(8,128)} %param.46) | copy-start | bytes 98308
  23.5 21.1 %copy-start.2 = (bf16[1,128,1024]{2,1,0:T(8,128)(2,1)S(1)}, bf16[1,128,1024]{2,1,0:T(8,128)(2,1)}, u32[]{:S(2)}) copy-start(bf16[1,128,1024]{2,1,0:T(8,128)(2,1)} %param.45) | copy-start | bytes 786436
  25.4 11.5 %all-to-all-start = ((bf16[4,2,128]{2,1,0:T(2,128)(2,1)}), bf16[4,2,128]{2,1,0:T(2,128)(2,1)S(1)}, u32[]{:S(2)}, u32[]{:S(2)}) async-start(bf16[4,2,128]{2,1,0:T(2,128)(2,1)} %reshape.385), calls=%async_computation | async-start | bytes 4096 | tf_op jit(solution)/shard_map/all_to_all | solution.py:87
  28.7 5.3 %copy-start.1 = (bf16[2048,16,32]{0,2,1:T(8,128)(2,1)S(1)}, bf16[2048,16,32]{0,2,1:T(8,128)(2,1)}, u32[]{:S(2)}) copy-start(bf16[2048,16,32]{0,2,1:T(8,128)(2,1)} %param.30) | copy-start | bytes 6291460
  34.1 34.9 %copy-start.6 = (bf16[1,3,64,32]{2,3,1,0:T(8,128)(2,1)S(1)}, bf16[1,3,64,32]{2,3,1,0:T(8,128)(2,1)}, u32[]{:S(2)}) copy-start(bf16[1,3,64,32]{2,3,1,0:T(8,128)(2,1)} %param.40) | copy-start | bytes 36868
  34.1 36.2 %copy-start.7 = (f32[64,32]{0,1:T(8,128)S(1)}, f32[64,32]{0,1:T(8,128)}, u32[]{:S(2)}) copy-start(f32[64,32]{0,1:T(8,128)} %param.48) | copy-start | bytes 24580
  35.6 8.4 %copy-start.8 = (f32[128]{0:T(128)}, f32[128]{0:T(128)S(1)}, u32[]{:S(2)}) copy-start(f32[128]{0:T(128)S(1)} %compare_convert_fusion) | copy-start | bytes 1540
  36.9 10.6 %all-to-all-start.1 = ((bf16[4,2,128]{2,1,0:T(2,128)(2,1)}), bf16[4,2,128]{2,1,0:T(2,128)(2,1)S(1)}, u32[]{:S(2)}, u32[]{:S(2)}) async-start(bf16[4,2,128]{2,1,0:T(2,128)(2,1)} %reshape.387), calls=%async_computation.1 | async-start | bytes 4096 | tf_op jit(solution)/shard_map/all_to_all | solution.py:86
  44.8 24.2 %copy-start.3 = (f32[4,64,32]{1,2,0:T(8,128)S(1)}, f32[4,64,32]{1,2,0:T(8,128)}, u32[]{:S(2)}) copy-start(f32[4,64,32]{1,2,0:T(8,128)} %param.37) | copy-start | bytes 98308
  47.5 10.7 %all-to-all-start.2 = ((bf16[4,2,256]{2,1,0:T(2,128)(2,1)}), bf16[4,2,256]{2,1,0:T(2,128)(2,1)S(1)}, u32[]{:S(2)}, u32[]{:S(2)}) async-start(bf16[4,2,256]{2,1,0:T(2,128)(2,1)} %reshape.383), calls=%async_computation.2 | async-start | bytes 8192 | tf_op jit(solution)/shard_map/all_to_all | solution.py:85
  50.8 58.5 %copy-start.4 = (f32[2048]{0:T(1024)S(1)}, f32[2048]{0:T(1024)}, u32[]{:S(2)}) copy-start(f32[2048]{0:T(1024)} %param.50) | copy-start | bytes 24580
  58.2 10.6 %all-to-all-start.3 = ((bf16[4,2,256]{2,1,0:T(2,128)(2,1)}), bf16[4,2,256]{2,1,0:T(2,128)(2,1)S(1)}, u32[]{:S(2)}, u32[]{:S(2)}) async-start(bf16[4,2,256]{2,1,0:T(2,128)(2,1)} %reshape.381), calls=%async_computation.3 | async-start | bytes 8192 | tf_op jit(solution)/shard_map/all_to_all | solution.py:84
  71.9 8.8 %all-to-all-start.4 = ((bf16[4,2,256]{2,1,0:T(2,128)(2,1)}), bf16[4,2,256]{2,1,0:T(2,128)(2,1)S(1)}, u32[]{:S(2)}, u32[]{:S(2)}) async-start(bf16[4,2,256]{2,1,0:T(2,128)(2,1)} %reshape.389), calls=%async_computation.4 | async-start | bytes 8192 | tf_op jit(solution)/shard_map/all_to_all | solution.py:138
  75.1 72.7 %reduce-scatter.4.cloned.1.call-start = ((), (), s32[]{:S(2)}) async-start(), calls=%async_computation.6 | async-start | bytes 1179648
Sparse Core Ops, SparseCore 0:
  117.0 30.8 reduce-scatter.3
where the time goes:
time: 157 us; the launch traced here: 156 us
  waiting for transfers between devices  42.1 us (27%)
  blocking collectives  41 us (26%)
  matrix products  20.9 us (13%)
  starting transfers between devices  20 us (13%)
  between operations  14.4 us (9%)
  other arithmetic  8.9 us (6%)
  local copies, waits for them, and re-layouts  8.85 us (6%)
    unnamed x2, waiting for transfers between devices  31 us
    psum x1, blocking collectives, shards(): lax.psum(jnp.einsum('hpd,shp->ds', columns, by_head, preferred_element_ty...  26.3 us
    all_gather x1, blocking collectives, shards(): whole_rows = lax.all_gather(hidden, ('kv', 'tp'), axis=0, tiled=True)  14.7 us
    unnamed x33, local copies, waits for them, and re-layouts  6.14 us
    all_to_all x1, starting transfers between devices, shards(): lax.all_to_all(input_part, 'kv', split_axis=0, concat_axis=1, tiled=True)  5.1 us
    all_to_all x1, starting transfers between devices, shards(): lax.all_to_all(gate_part, 'kv', split_axis=0, concat_axis=1, tiled=True)  5.06 us
    all_to_all x1, waiting for transfers between devices, shards(): lax.all_to_all(gated, 'kv', split_axis=1, concat_axis=0, tiled=True)  4.73 us
    all_to_all x1, waiting for transfers between devices, shards(): lax.all_to_all(gate_part, 'kv', split_axis=0, concat_axis=1, tiled=True)  3.87 us
  transfers between devices with their start and end apart: 6, of which 4 were waited for; matrix products, arithmetic and copies ran while one was open for 13% of the time, Pallas kernels for 0%

commit v1 on v0

--- a/solution.py
+++ b/solution.py
@@ -138,8 +138,10 @@
     by_head = lax.all_to_all(gated, "kv", split_axis=1, concat_axis=0, tiled=True)
     columns = mixer_out
     mixed_full = rms_gate[None, :] * lax.psum(
-        jnp.einsum("hpd,shp->ds", columns, by_head, preferred_element_type=jnp.float32),
-        ("kv", "tp"),
+        lax.psum(
+            jnp.einsum("hpd,shp->ds", columns, by_head, preferred_element_type=jnp.float32), "tp"
+        ),
+        "kv",
     )
     mid_full = (whole_f + mixed_full).astype(jnp.bfloat16)
     mid = lax.dynamic_slice_in_dim(mid_full, offset, rows_own, 0)

time: 157 us -> 166 us (1.057)
  blocking collectives: 41 us -> 48 us
    psum x0 -> x2, blocking collectives: none -> 29.9 us  [the longest x1 16.2 us: shards(): lax.psum(lax.psum(jnp.einsum('hpd,shp->ds', columns, by_head, preferred_e...]
    psum x1, blocking collectives: 26.3 us -> 3.4 us  [shards(): lax.psum(jnp.einsum('hpd,shp->ds', columns, by_head, preferred_element_ty...]
  transfers between devices with their start and end apart: 6 -> 6, of which waited for: 4 -> 4; matrix products, arithmetic and copies ran while one was open for 13% -> 12% of each run, Pallas kernels for 0% -> 0%
where the time goes in v1:
time: 166 us; the launch traced here: 165 us
  blocking collectives  48 us (29%)
  waiting for transfers between devices  43.7 us (26%)
  matrix products  20.9 us (13%)
  starting transfers between devices  20 us (12%)
  between operations  14.4 us (9%)
  other arithmetic  8.89 us (5%)
  local copies, waits for them, and re-layouts  8.84 us (5%)
    unnamed x2, waiting for transfers between devices  31.8 us
    psum x1, blocking collectives, shards(): lax.psum(lax.psum(jnp.einsum('hpd,shp->ds', columns, by_head, preferred_e...  16.2 us
    all_gather x1, blocking collectives, shards(): whole_rows = lax.all_gather(hidden, ('kv', 'tp'), axis=0, tiled=True)  14.7 us
    psum x1, blocking collectives, shards(): gate_squares = lax.psum(placed, ('kv', 'tp'))  13.6 us
    unnamed x33, local copies, waits for them, and re-layouts  6.14 us
    all_to_all x1, waiting for transfers between devices, shards(): lax.all_to_all(gated, 'kv', split_axis=1, concat_axis=0, tiled=True)  5.48 us
    all_to_all x1, starting transfers between devices, shards(): lax.all_to_all(input_part, 'kv', split_axis=0, concat_axis=1, tiled=True)  5.1 us
    all_to_all x1, starting transfers between devices, shards(): lax.all_to_all(gate_part, 'kv', split_axis=0, concat_axis=1, tiled=True)  5.06 us
  transfers between devices with their start and end apart: 6, of which 4 were waited for; matrix products, arithmetic and copies ran while one was open for 12% of the time, Pallas kernels for 0%

profile of v1, /device:TPU:0, one launch (start us, length us, event | category | flops | bytes accessed | tf_op | source)
XLA Modules:
  0.0 164.8 jit_solution(403082110130672706)
XLA Ops:
  6.5 14.7 %all_gather.3 = bf16[2048,4]{0,1:T(4,128)(2,1)S(1)} all-gather(bf16[256,4]{0,1:T(4,128)(2,1)} %param.27), channel_id=1, replica_groups=mesh['dp'=4,'kv'=4,'tp'=2] {'kv','tp'}, dimensions={0}, use_global_device_ids=true | all-gather | bytes 18432 | tf_op jit(solution)/shard_map/all_gather | solution.py:57
  21.3 0.8 fusion.15
  22.1 1.4 fusion.7
  25.4 3.4 %all-to-all-start = ((bf16[4,2,128]{2,1,0:T(2,128)(2,1)}), bf16[4,2,128]{2,1,0:T(2,128)(2,1)S(1)}, u32[]{:S(2)}, u32[]{:S(2)}) async-start(bf16[4,2,128]{2,1,0:T(2,128)(2,1)} %reshape.385), calls=%async_computation | async-start | bytes 4096 | tf_op jit(solution)/shard_map/all_to_all | solution.py:87
  29.5 1.4 fusion.6
  31.0 3.1 %fusion.1 = bf16[4,16,32]{2,0,1:T(4,128)(2,1)S(1)} fusion(bf16[2048,16,32]{0,2,1:T(8,128)(2,1)} %param.29, bf16[2048,4]{0,1:T(4,128)(2,1)S(1)} %get-tuple-element.14, f32[4]{0:T(128)S(1)} %add_rsqrt_fusion.2), kind=kOutput, calls=%fused_computation.5 | convolution fusion | flops 8392704 | bytes 2117648 | tf_op jit(solution)/shard_map/ds,dhp->shp/dot_general | solution.py:63
  34.1 1.5 fusion
  36.9 5.1 %all-to-all-start.1 = ((bf16[4,2,128]{2,1,0:T(2,128)(2,1)}), bf16[4,2,128]{2,1,0:T(2,128)(2,1)S(1)}, u32[]{:S(2)}, u32[]{:S(2)}) async-start(bf16[4,2,128]{2,1,0:T(2,128)(2,1)} %reshape.387), calls=%async_computation.1 | async-start | bytes 4096 | tf_op jit(solution)/shard_map/all_to_all | solution.py:86
  43.3 0.7 reshape.381
  45.0 2.5 %all-to-all-done.1 = bf16[4,2,128]{2,1,0:T(2,128)(2,1)S(1)} async-done(((bf16[4,2,128]{2,1,0:T(2,128)(2,1)}), bf16[4,2,128]{2,1,0:T(2,128)(2,1)S(1)}, u32[]{:S(2)}, u32[]{:S(2)}) %all-to-all-start.1) | async-done | bytes 2080 | tf_op jit(solution)/shard_map/all_to_all | solution.py:86
  47.5 3.2 %all-to-all-start.2 = ((bf16[4,2,256]{2,1,0:T(2,128)(2,1)}), bf16[4,2,256]{2,1,0:T(2,128)(2,1)S(1)}, u32[]{:S(2)}, u32[]{:S(2)}) async-start(bf16[4,2,256]{2,1,0:T(2,128)(2,1)} %reshape.383), calls=%async_computation.2 | async-start | bytes 8192 | tf_op jit(solution)/shard_map/all_to_all | solution.py:85
  50.8 0.8 multiply_reduce_fusion.3
  52.2 3.4 %fusion.43 = f32[8,1,8,32]{3,1,2,0:T(1,128)S(1)} fusion(f32[8,8,32,128]{3,2,1,0:T(8,128)} %bitcast.136, bf16[8,128,1,1]{1,0,2,3:T(8,128)(2,1)S(1)} %get-tuple-element.15), kind=kOutput, calls=%fused_computation.72 | convolution fusion | flops 3145728 | bytes 1058816 | tf_op jit(solution)/shard_map/sgn,sgrpn->sgrp/dot_general | solution.py:118
  55.5 1.8 %fusion.57 = (f32[64]{0:T(128)S(1)}, f32[64]{0:T(128)S(1)}, f32[64]{0:T(128)S(1)}) fusion(f32[64]{0:T(128)} %get-tuple-element.11, f32[64]{0:T(128)} %param.35, f32[64]{0:T(128)S(1)} %broadcast_in_dim.11, f32[64]{0:T(128)} %param.34, bf16[2048,64]{0,1:T(8,128)(2,1)} %param.33, bf16[2048,4]{0,1:T(4,128)(2,1)S(1)} %get-tuple-element.14, s32[]{:T(128)S(6)} %select_n.13, ...), kind=kOutput, calls=%fused_computation.90 | convolution fusion | flops 263040 | bytes 272392 | tf_op jit(solution)/shard_map/ds,dh->sh/dot_general | solution.py:81
  57.3 0.8 fusion.19
  58.2 5.1 %all-to-all-start.3 = ((bf16[4,2,256]{2,1,0:T(2,128)(2,1)}), bf16[4,2,256]{2,1,0:T(2,128)(2,1)S(1)}, u32[]{:S(2)}, u32[]{:S(2)}) async-start(bf16[4,2,256]{2,1,0:T(2,128)(2,1)} %reshape.381), calls=%async_computation.3 | async-start | bytes 8192 | tf_op jit(solution)/shard_map/all_to_all | solution.py:84
  63.2 1.4 multiply_reduce_fusion
  65.0 3.9 %all-to-all-done.3 = bf16[4,2,256]{2,1,0:T(2,128)(2,1)S(1)} async-done(((bf16[4,2,256]{2,1,0:T(2,128)(2,1)}), bf16[4,2,256]{2,1,0:T(2,128)(2,1)S(1)}, u32[]{:S(2)}, u32[]{:S(2)}) %all-to-all-start.3) | async-done | bytes 4128 | tf_op jit(solution)/shard_map/all_to_all | solution.py:84
  69.0 1.3 multiply_reduce_fusion.2
  70.3 0.8 dynamic_update_slice.3
  71.1 13.6 %psum.21 = f32[4]{0:T(128)S(1)} all-reduce(f32[4]{0:T(128)S(1)} %dynamic_update_slice.3), channel_id=1, replica_groups=mesh['dp'=4,'kv'=4,'tp'=2] {'kv','tp'}, use_global_device_ids=true, to_apply=%region_8.9 | all-reduce | flops 4 | bytes 32 | tf_op jit(solution)/shard_map/psum | solution.py:136
  84.8 0.7 reduce.14
  86.3 3.2 %all-to-all-start.4 = ((bf16[4,2,256]{2,1,0:T(2,128)(2,1)}), bf16[4,2,256]{2,1,0:T(2,128)(2,1)S(1)}, u32[]{:S(2)}, u32[]{:S(2)}) async-start(bf16[4,2,256]{2,1,0:T(2,128)(2,1)} %reshape.389), calls=%async_computation.4 | async-start | bytes 8192 | tf_op jit(solution)/shard_map/all_to_all | solution.py:138
  89.6 5.5 %all-to-all-done.4 = bf16[4,2,256]{2,1,0:T(2,128)(2,1)S(1)} async-done(((bf16[4,2,256]{2,1,0:T(2,128)(2,1)}), bf16[4,2,256]{2,1,0:T(2,128)(2,1)S(1)}, u32[]{:S(2)}, u32[]{:S(2)}) %all-to-all-start.4) | async-done | bytes 4128 | tf_op jit(solution)/shard_map/all_to_all | solution.py:138
  95.2 2.0 %convolution_bitcast_fusion.1 = f32[2048,4]{0,1:T(4,128)S(1)} fusion(bf16[16,32,2048]{2,1,0:T(8,128)(2,1)} %param.49, bf16[4,16,32]{2,1,0:T(8,128)(2,1)S(1)} %bitcast.141), kind=kOutput, calls=%fused_computation.1 | convolution fusion | flops 8388608 | bytes 2134016 | tf_op jit(solution)/shard_map/hpd,shp->ds/dot_general | solution.py:142
  97.2 3.4 %psum.22 = f32[2048,4]{0,1:T(4,128)S(1)} all-reduce(f32[2048,4]{0,1:T(4,128)S(1)} %convolution_bitcast_fusion.1), channel_id=1, replica_groups=mesh['dp'=4,'kv'=4,'tp'=2] {'tp'}, use_global_device_ids=true, to_apply=%region_9.10 | all-reduce | flops 8192 | bytes 65536 | tf_op jit(solution)/shard_map/psum | solution.py:141
  100.6 16.2 %psum.23 = f32[2048,4]{0,1:T(4,128)S(1)} all-reduce(f32[2048,4]{0,1:T(4,128)S(1)} %psum.22), channel_id=1, replica_groups=mesh['dp'=4,'kv'=4,'tp'=2] {'kv'}, use_global_device_ids=true, to_apply=%region_10.11 | all-reduce | flops 8192 | bytes 65536 | tf_op jit(solution)/shard_map/psum | solution.py:140
  117.1 2.7 %convolution_multiply_fusion.3 = f32[4,704]{1,0:T(4,128)S(1)} fusion(bf16[2048,704]{0,1:T(8,128)(2,1)} %param.51, bf16[2048,4]{0,1:T(4,128)(2,1)S(1)} %get-tuple-element.6, f32[2048]{0:T(1024)S(1)} %copy-done.4, f32[4]{0:T(128)S(1)} %add_rsqrt_fusion), kind=kOutput, calls=%fused_computation.8 | convolution fusion | flops 11561728 | bytes 2919440 | tf_op jit(solution)/shard_map/ds,df->sf/dot_general | solution.py:151
  119.7 3.5 %convolution_bitcast_fusion = f32[2048,4]{0,1:T(4,128)S(1)} fusion(bf16[704,2048]{1,0:T(8,128)(2,1)S(1)} %copy-done, bf16[2048,704]{0,1:T(8,128)(2,1)} %param.52, f32[4,704]{1,0:T(4,128)S(1)} %convolution_multiply_fusion.3, bf16[2048,4]{0,1:T(4,128)(2,1)S(1)} %get-tuple-element.6, f32[2048]{0:T(1024)S(1)} %copy-done.4, f32[4]{0:T(128)S(1)} %add_rsqrt_fusion), kind=kOutput, calls=%fused_computation | convolution fusion | flops 23112960 | bytes 5835792 | tf_op jit(solution)/shard_map/fd,sf->ds/dot_general | solution.py:161
  123.2 1.4 copy.71
  124.6 31.8 %reduce-scatter.4.cloned.1.call-done = f32[256,4]{1,0:T(8,128)} async-done(((f32[2048,4]{1,0:T(8,128)}), f32[256,4]{1,0:T(8,128)}) %reduce-scatter.4.cloned.1.call-update) | async-done | bytes 4112
  156.4 1.0 copy.72
  (65 shorter events, 8.4 us)
Async XLA Ops:
  6.5 113.2 %copy-start = (bf16[704,2048]{1,0:T(8,128)(2,1)S(1)}, bf16[704,2048]{1,0:T(8,128)(2,1)}, u32[]{:S(2)}) copy-start(bf16[704,2048]{1,0:T(8,128)(2,1)} %param.53) | copy-start | bytes 8650756
  23.5 13.3 %copy-start.5 = (f32[1,128,64]{1,2,0:T(8,128)S(1)}, f32[1,128,64]{1,2,0:T(8,128)}, u32[]{:S(2)}) copy-start(f32[1,128,64]{1,2,0:T(8,128)} %param.46) | copy-start | bytes 98308
  23.5 21.1 %copy-start.2 = (bf16[1,128,1024]{2,1,0:T(8,128)(2,1)S(1)}, bf16[1,128,1024]{2,1,0:T(8,128)(2,1)}, u32[]{:S(2)}) copy-start(bf16[1,128,1024]{2,1,0:T(8,128)(2,1)} %param.45) | copy-start | bytes 786436
  25.4 11.5 %all-to-all-start = ((bf16[4,2,128]{2,1,0:T(2,128)(2,1)}), bf16[4,2,128]{2,1,0:T(2,128)(2,1)S(1)}, u32[]{:S(2)}, u32[]{:S(2)}) async-start(bf16[4,2,128]{2,1,0:T(2,128)(2,1)} %reshape.385), calls=%async_computation | async-start | bytes 4096 | tf_op jit(solution)/shard_map/all_to_all | solution.py:87
  28.7 5.3 %copy-start.1 = (bf16[2048,16,32]{0,2,1:T(8,128)(2,1)S(1)}, bf16[2048,16,32]{0,2,1:T(8,128)(2,1)}, u32[]{:S(2)}) copy-start(bf16[2048,16,32]{0,2,1:T(8,128)(2,1)} %param.30) | copy-start | bytes 6291460
  34.1 34.9 %copy-start.6 = (bf16[1,3,64,32]{2,3,1,0:T(8,128)(2,1)S(1)}, bf16[1,3,64,32]{2,3,1,0:T(8,128)(2,1)}, u32[]{:S(2)}) copy-start(bf16[1,3,64,32]{2,3,1,0:T(8,128)(2,1)} %param.40) | copy-start | bytes 36868
  34.1 50.6 %copy-start.7 = (f32[64,32]{0,1:T(8,128)S(1)}, f32[64,32]{0,1:T(8,128)}, u32[]{:S(2)}) copy-start(f32[64,32]{0,1:T(8,128)} %param.48) | copy-start | bytes 24580
  35.6 8.4 %copy-start.8 = (f32[128]{0:T(128)}, f32[128]{0:T(128)S(1)}, u32[]{:S(2)}) copy-start(f32[128]{0:T(128)S(1)} %compare_convert_fusion) | copy-start | bytes 1540
  36.9 10.6 %all-to-all-start.1 = ((bf16[4,2,128]{2,1,0:T(2,128)(2,1)}), bf16[4,2,128]{2,1,0:T(2,128)(2,1)S(1)}, u32[]{:S(2)}, u32[]{:S(2)}) async-start(bf16[4,2,128]{2,1,0:T(2,128)(2,1)} %reshape.387), calls=%async_computation.1 | async-start | bytes 4096 | tf_op jit(solution)/shard_map/all_to_all | solution.py:86
  44.8 24.2 %copy-start.3 = (f32[4,64,32]{1,2,0:T(8,128)S(1)}, f32[4,64,32]{1,2,0:T(8,128)}, u32[]{:S(2)}) copy-start(f32[4,64,32]{1,2,0:T(8,128)} %param.37) | copy-start | bytes 98308
  47.5 10.6 %all-to-all-start.2 = ((bf16[4,2,256]{2,1,0:T(2,128)(2,1)}), bf16[4,2,256]{2,1,0:T(2,128)(2,1)S(1)}, u32[]{:S(2)}, u32[]{:S(2)}) async-start(bf16[4,2,256]{2,1,0:T(2,128)(2,1)} %reshape.383), calls=%async_computation.2 | async-start | bytes 8192 | tf_op jit(solution)/shard_map/all_to_all | solution.py:85
  51.8 65.3 %copy-start.4 = (f32[2048]{0:T(1024)S(1)}, f32[2048]{0:T(1024)}, u32[]{:S(2)}) copy-start(f32[2048]{0:T(1024)} %param.50) | copy-start | bytes 24580
  58.2 10.6 %all-to-all-start.3 = ((bf16[4,2,256]{2,1,0:T(2,128)(2,1)}), bf16[4,2,256]{2,1,0:T(2,128)(2,1)S(1)}, u32[]{:S(2)}, u32[]{:S(2)}) async-start(bf16[4,2,256]{2,1,0:T(2,128)(2,1)} %reshape.381), calls=%async_computation.3 | async-start | bytes 8192 | tf_op jit(solution)/shard_map/all_to_all | solution.py:84
  86.3 8.8 %all-to-all-start.4 = ((bf16[4,2,256]{2,1,0:T(2,128)(2,1)}), bf16[4,2,256]{2,1,0:T(2,128)(2,1)S(1)}, u32[]{:S(2)}, u32[]{:S(2)}) async-start(bf16[4,2,256]{2,1,0:T(2,128)(2,1)} %reshape.389), calls=%async_computation.4 | async-start | bytes 8192 | tf_op jit(solution)/shard_map/all_to_all | solution.py:138
  89.5 66.9 %reduce-scatter.4.cloned.1.call-start = ((), (), s32[]{:S(2)}) async-start(), calls=%async_computation.6 | async-start | bytes 1179648
Sparse Core Ops, SparseCore 0:
  124.7 31.6 reduce-scatter.3
